TPU v7x, 32 devices: a whole 2x2x4 slice. The times are simulated.
32 devices in a mesh: kv: 8 (over z, y), tp: 4 (over x, core).
Axes of the slice: x: 2, y: 2, z: 4, core: 2. Of those that a mesh axis runs over, the one named last changes fastest.
Arguments:
- stream: bfloat16 [32, 4096], P(None, ('kv', 'tp')), may hold values from -60 to 60
- memory_state: float32 [32, 32, 128, 128], P('kv', 'tp'), may hold values from -3 to 3
- attn_gain: float32 [4096], P('kv'), may hold values from 0.1 to 1.9
- query_weight: bfloat16 [4096, 4096], P('kv', 'tp'), may hold values from -0.09375 to 0.09375
- key_weight: bfloat16 [4096, 4096], P('kv', 'tp'), may hold values from -0.09375 to 0.09375
- value_weight: bfloat16 [4096, 4096], P('kv', 'tp'), may hold values from -0.09375 to 0.09375
- outgate_weight: bfloat16 [4096, 4096], P('kv', 'tp'), may hold values from -0.09375 to 0.09375
- beta_weight: bfloat16 [4096, 32], P('kv', 'tp'), may hold values from -0.09375 to 0.09375
- decay_weight: bfloat16 [4096, 32], P('kv', 'tp'), may hold values from -0.09375 to 0.09375
- decay_log: float32 [32], P('tp'), may hold values from -4 to 1
- decay_shift: float32 [32], P('tp'), may hold values from -3 to 3
- head_gain: float32 [128], replicated, may hold values from 0.1 to 1.9
- output_weight: bfloat16 [4096, 4096], P('tp', 'kv'), may hold values from -0.09375 to 0.09375
- mixer_gain: float32 [4096], P('kv'), may hold values from 0.1 to 1.9
- up_weight: bfloat16 [4096, 16384], P('kv', 'tp'), may hold values from -0.09375 to 0.09375
- down_weight: bfloat16 [16384, 4096], P('tp', 'kv'), may hold values from -0.046875 to 0.046875
Outputs:
- layer_out: bfloat16 [32, 4096], P(None, ('kv', 'tp'))
- memory_next: float32 [32, 32, 128, 128], P('kv', 'tp')
All inputs are finite; a program needn't handle non-finite values.
Results may differ from a plain program's by a relative error of at most 0.025.
Values may be sent and summed in bfloat16 or wider, within the bound.
A program may use at most 64 MiB of HBM per device.

v0:
```python
import jax
import jax.numpy as jnp
from jax import lax
from jax.sharding import PartitionSpec as P

D = 4096
HEAD_DIM = 128


epsilon = 1e-06


def gathered_rows(stream, gain_vec):
    gathered = lax.all_gather(stream, "tp", axis=1, tiled=True)
    widened = gathered.astype(jnp.float32)
    squares = jnp.sum(widened * widened, axis=1)
    scaled = (widened * gain_vec).astype(jnp.bfloat16)
    return (scaled, squares)


def unit_rows(values):
    return values * lax.rsqrt(jnp.sum(values * values, axis=-1, keepdims=True) + epsilon)


def head_output(
    memory_state,
    query_sum,
    key_sum,
    value_sum,
    gate_sum,
    beta_sum,
    decay_sum,
    decay_log,
    decay_shift,
    head_gain,
):
    row_count = query_sum.shape[0]
    head_count = beta_sum.shape[1]

    def to_heads(values):
        return values.reshape(row_count, head_count, HEAD_DIM)

    query_heads = unit_rows(jax.nn.silu(to_heads(query_sum))) * HEAD_DIM ** (-0.5)
    key_heads = unit_rows(jax.nn.silu(to_heads(key_sum)))
    value_heads = jax.nn.silu(to_heads(value_sum))
    beta_heads = jax.nn.sigmoid(beta_sum)
    decay_heads = jnp.exp(-jnp.exp(decay_log) * jax.nn.softplus(decay_sum + decay_shift))
    kept_state = memory_state * decay_heads[:, :, None, None]
    recalled = jnp.einsum("bhkv,bhk->bhv", kept_state, key_heads)
    correction = beta_heads[:, :, None] * (value_heads - recalled)
    memory_next = kept_state + key_heads[:, :, :, None] * correction[:, :, None, :]
    readout = jnp.einsum("bhkv,bhk->bhv", memory_next, query_heads)
    normed = readout * lax.rsqrt(jnp.mean(readout * readout, axis=-1, keepdims=True) + epsilon)
    gated = normed * head_gain * jax.nn.silu(to_heads(gate_sum))
    return (gated.reshape(row_count, head_count * HEAD_DIM).astype(jnp.bfloat16), memory_next)


def shards(
    stream,
    memory_state,
    attn_gain,
    query_weight,
    key_weight,
    value_weight,
    outgate_weight,
    beta_weight,
    decay_weight,
    decay_log,
    decay_shift,
    head_gain,
    output_weight,
    mixer_gain,
    up_weight,
    down_weight,
):
    scaled, squares = gathered_rows(stream, attn_gain)

    def product(weight):
        return jnp.dot(scaled, weight, preferred_element_type=jnp.float32)

    query_sum, key_sum, value_sum, gate_sum, beta_sum, decay_sum, own_squares = (
        lax.psum_scatter(product(query_weight), "kv", scatter_dimension=0, tiled=True),
        lax.psum_scatter(product(key_weight), "kv", scatter_dimension=0, tiled=True),
        lax.psum_scatter(product(value_weight), "kv", scatter_dimension=0, tiled=True),
        lax.psum_scatter(product(outgate_weight), "kv", scatter_dimension=0, tiled=True),
        lax.psum_scatter(product(beta_weight), "kv", scatter_dimension=0, tiled=True),
        lax.psum_scatter(product(decay_weight), "kv", scatter_dimension=0, tiled=True),
        lax.psum_scatter(squares, "kv", scatter_dimension=0, tiled=True),
    )
    factor = lax.rsqrt(own_squares / D + epsilon)[:, None]
    heads_out, memory_next = head_output(
        memory_state,
        query_sum * factor,
        key_sum * factor,
        value_sum * factor,
        gate_sum * factor,
        beta_sum * factor,
        decay_sum * factor,
        decay_log,
        decay_shift,
        head_gain,
    )
    attn_rows = jnp.dot(
        lax.all_gather(heads_out, "kv", axis=0, tiled=True),
        output_weight,
        preferred_element_type=jnp.float32,
    )
    attn_mine = lax.psum_scatter(attn_rows, "tp", scatter_dimension=1, tiled=True)
    middle = (stream.astype(jnp.float32) + attn_mine).astype(jnp.bfloat16)
    scaled_mix, squares_mix = gathered_rows(middle, mixer_gain)
    up_part = jnp.dot(scaled_mix, up_weight, preferred_element_type=jnp.float32)
    up_total, square_total = (
        lax.psum(up_part.astype(jnp.bfloat16), "kv").astype(jnp.float32),
        lax.psum(squares_mix.astype(jnp.bfloat16), "kv").astype(jnp.float32),
    )
    hidden = jnp.square(
        jax.nn.relu(up_total * lax.rsqrt(square_total / D + epsilon)[:, None])
    ).astype(jnp.bfloat16)
    down_rows = jnp.dot(hidden, down_weight, preferred_element_type=jnp.float32)
    mixer_mine = lax.psum_scatter(
        down_rows.astype(jnp.bfloat16), "tp", scatter_dimension=1, tiled=True
    ).astype(jnp.float32)
    layer_out = (middle.astype(jnp.float32) + mixer_mine).astype(jnp.bfloat16)
    return (layer_out, memory_next)


def solution(mesh):
    in_specs = (
        P(None, ("kv", "tp")),
        P("kv", "tp", None, None),
        P("kv"),
        P("kv", "tp"),
        P("kv", "tp"),
        P("kv", "tp"),
        P("kv", "tp"),
        P("kv", "tp"),
        P("kv", "tp"),
        P("tp"),
        P("tp"),
        P(),
        P("tp", "kv"),
        P("kv"),
        P("kv", "tp"),
        P("tp", "kv"),
    )
    out_specs = (P(None, ("kv", "tp")), P("kv", "tp", None, None))
    return jax.shard_map(shards, mesh=mesh, in_specs=in_specs, out_specs=out_specs, check_vma=False)
```

profile of v0, /device:TPU:0, one launch (start us, length us, event | category | flops | bytes accessed | tf_op | source)
XLA Modules:
  0.0 261.7 jit_solution(8634142251092570144)
XLA Ops:
  7.2 0.0 copy-start
  7.2 0.0 copy-start.6
  7.2 0.0 all-reduce.14.cloned.1.call-start
  7.2 0.0 copy-start.3
  7.2 0.0 copy-start.4
  7.3 6.5 %all_gather.9 = bf16[32,512]{1,0:T(8,128)(2,1)S(1)} all-gather(bf16[32,128]{1,0:T(8,128)(2,1)} %param.16), channel_id=1, replica_groups=mesh['kv'=8,'tp'=4] {'tp'}, dimensions={1}, use_global_device_ids=true | all-gather | bytes 40960 | tf_op jit(solution)/shard_map/all_gather | solution.py:14
  13.7 0.0 copy-done
  13.7 1.6 fusion.39
  15.4 0.0 copy-start.12
  15.4 0.0 copy-start.1
  15.4 2.3 fusion.35
  17.7 0.0 copy-done.6
  17.7 0.0 copy-done.3
  17.7 1.0 fusion.33
  18.7 0.0 copy-done.4
  18.7 0.9 fusion.31
  19.7 0.0 all-reduce.14.cloned.1.call-update
  19.7 0.0 reduce-scatter.5.cloned.1.call-start
  19.7 0.1 fusion.6
  19.9 0.0 copy-done.8
  19.9 0.1 fusion.37
  20.0 0.1 fusion.41
  20.1 0.6 dynamic-slice
  21.4 38.5 %all-reduce.7 = (f32[32]{0:T(128)S(1)}, f32[32,8]{1,0:T(8,128)S(1)}, f32[32,8]{1,0:T(8,128)S(1)}) all-reduce(f32[32]{0:T(128)S(1)} %fusion.6, f32[32,8]{1,0:T(8,128)S(1)} %fusion.41, f32[32,8]{1,0:T(8,128)S(1)} %fusion.37), channel_id=3, replica_groups=mesh['kv'=8,'tp'=4] {'kv'}, use_global_device_ids=true, to_apply=%region_2.0.clone | all-reduce | flops 544 | bytes 4352
  59.8 0.1 fusion.51
  59.9 0.0 copy-done.13
  59.9 0.1 fusion.48
  60.0 35.2 %all-reduce.14.cloned.1.call-done = (f32[32,1024]{1,0:T(8,128)}, f32[32,1024]{1,0:T(8,128)}, f32[32,1024]{1,0:T(8,128)}, f32[32,1024]{1,0:T(8,128)}) async-done(((f32[32,1024]{1,0:T(8,128)}, f32[32,1024]{1,0:T(8,128)}, f32[32,1024]{1,0:T(8,128)}, f32[32,1024]{1,0:T(8,128)}), (f32[32,1024]{1,0:T(8,128)}, f32[32,1024]{1,0:T(8,128)}, f32[32,1024]{1,0:T(8,128)}, ...) | async-done | bytes 524304
  95.2 0.9 fusion.27
  96.1 0.1 multiply_reduce_fusion.1
  96.2 0.1 multiply_reduce_fusion.2
  96.3 0.1 broadcast_multiply_fusion
  96.4 0.5 fusion
  96.9 0.1 fusion.22
  96.9 0.7 multiply_add_fusion
  97.7 0.0 copy-start.2
  97.7 0.0 copy-start.11
  97.7 0.0 copy-start.5
  97.7 0.0 copy-start.7
  97.8 0.0 copy-start.10
  97.8 1.3 copy-done.2
  99.0 0.4 fusion.53
  99.4 0.1 multiply_reduce_fusion
  99.5 0.1 fusion.30
  99.6 30.5 %all-gather = bf16[8,4,1024]{2,1,0:T(4,128)(2,1)S(1)} all-gather(bf16[1,4,1024]{2,1,0:T(4,128)(2,1)S(1)} %reshape.65), channel_id=1, replica_groups=mesh['kv'=8,'tp'=4] {'kv'}, dimensions={0}, use_global_device_ids=true | all-gather | bytes 73728 | tf_op jit(solution)/shard_map/all_gather | solution.py:104
  130.2 0.9 fusion.54
  131.1 0.0 reduce-scatter.5.cloned.1.call-update
  131.1 0.0 all-reduce.12.cloned.1.call-start
  131.2 18.8 %reduce-scatter.5.cloned.1.call-done = f32[32,128]{1,0:T(8,128)} async-done(((f32[32,512]{1,0:T(8,128)}), f32[32,128]{1,0:T(8,128)}) %reduce-scatter.5.cloned.1.call-update) | async-done | bytes 16400 | tf_op jit(solution)/shard_map/reduce_scatter | solution.py:108
  149.9 0.0 copy-done.7
  149.9 0.7 add_convert_fusion.1
  150.6 5.2 %all_gather.11 = bf16[32,512]{1,0:T(8,128)(2,1)S(1)} all-gather(bf16[32,128]{1,0:T(8,128)(2,1)S(1)} %add_convert_fusion.1), channel_id=1, replica_groups=mesh['kv'=8,'tp'=4] {'tp'}, dimensions={1}, use_global_device_ids=true | all-gather | bytes 40960 | tf_op jit(solution)/shard_map/all_gather | solution.py:14
  155.8 3.7 %convolution_convert_fusion = bf16[32,4096]{1,0:T(8,128)(2,1)} fusion(bf16[512,4096]{1,0:T(8,128)(2,1)} %param.30, bf16[32,512]{1,0:T(8,128)(2,1)S(1)} %all_gather.11, f32[512]{0:T(512)S(1)} %copy-done.10), kind=kOutput, calls=%fused_computation | convolution fusion | flops 134397952 | bytes 4491264 | tf_op jit(solution)/shard_map/dot_general | solution.py:111
  159.5 0.0 all-reduce.12.cloned.1.call-update
  159.5 0.0 reduce-scatter.7.cloned.1.call-start
  159.6 0.1 fusion.8
  159.7 21.4 %psum.15 = bf16[32]{0:T(256)(128)(2,1)S(1)} all-reduce(bf16[32]{0:T(256)(128)(2,1)S(1)} %fusion.8), channel_id=1, replica_groups=mesh['kv'=8,'tp'=4] {'kv'}, use_global_device_ids=true, to_apply=%region_14.15 | all-reduce | flops 32 | bytes 128 | tf_op jit(solution)/shard_map/psum | solution.py:114
  181.1 49.6 %all-reduce.12.cloned.1.call-done = bf16[32,4096]{1,0:T(8,128)(2,1)} async-done(((bf16[32,4096]{1,0:T(8,128)(2,1)}), bf16[32,4096]{1,0:T(8,128)(2,1)}) %all-reduce.12.cloned.1.call-update) | async-done | bytes 262160 | tf_op jit(solution)/shard_map/psum | solution.py:113
  230.8 3.2 %convolution_convert_fusion.1 = bf16[32,512]{1,0:T(8,128)(2,1)S(1)} fusion(bf16[4096,512]{1,0:T(8,128)(2,1)} %param.31, bf16[32,4096]{1,0:T(8,128)(2,1)} %all-reduce.12.cloned.1.call-done, f32[32]{0:T(128)S(1)} %add_rsqrt_fusion.3), kind=kOutput, calls=%fused_computation.4 | convolution fusion | flops 134889472 | bytes 4489344 | tf_op jit(solution)/shard_map/dot_general | solution.py:119
  233.9 0.8 copy.22
  234.7 0.0 reduce-scatter.7.cloned.1.call-update
  234.7 19.0 %reduce-scatter.7.cloned.1.call-done = bf16[128,32]{1,0:T(8,128)(2,1)} async-done(((bf16[512,32]{1,0:T(8,128)(2,1)}), bf16[128,32]{1,0:T(8,128)(2,1)}) %reduce-scatter.7.cloned.1.call-update) | async-done | bytes 8208
  253.7 0.8 copy.23
  254.5 0.6 add_convert_fusion
  (18 shorter events, 0.1 us)
Async XLA Ops:
  7.2 6.6 %copy-start = (bf16[512,1024]{1,0:T(8,128)(2,1)S(1)}, bf16[512,1024]{1,0:T(8,128)(2,1)}, u32[]{:S(2)}) copy-start(bf16[512,1024]{1,0:T(8,128)(2,1)} %param.20) | copy-start | bytes 3145732
  7.2 10.6 %copy-start.6 = (f32[512]{0:T(512)S(1)}, f32[512]{0:T(512)}, u32[]{:S(2)}) copy-start(f32[512]{0:T(512)} %param.18) | copy-start | bytes 6148
  7.2 88.0 %all-reduce.14.cloned.1.call-start = ((), (), s32[]{:S(2)}) async-start(), calls=%async_computation.5 | async-start | bytes 1048576
  7.2 10.5 %copy-start.3 = (bf16[512,1024]{1,0:T(8,128)(2,1)S(1)}, bf16[512,1024]{1,0:T(8,128)(2,1)}, u32[]{:S(2)}) copy-start(bf16[512,1024]{1,0:T(8,128)(2,1)} %param.19) | copy-start | bytes 3145732
  7.2 11.5 %copy-start.4 = (bf16[512,1024]{1,0:T(8,128)(2,1)S(1)}, bf16[512,1024]{1,0:T(8,128)(2,1)}, u32[]{:S(2)}) copy-start(bf16[512,1024]{1,0:T(8,128)(2,1)} %param.22) | copy-start | bytes 3145732
  15.4 4.5 %copy-start.8 = (bf16[512,8]{0,1:T(8,128)(2,1)S(1)}, bf16[512,8]{0,1:T(8,128)(2,1)}, u32[]{:S(2)}) copy-start(bf16[512,8]{0,1:T(8,128)(2,1)} %param.23) | copy-start | bytes 24580
  15.4 4.6 %copy-start.9 = (bf16[512,8]{0,1:T(8,128)(2,1)S(1)}, bf16[512,8]{0,1:T(8,128)(2,1)}, u32[]{:S(2)}) copy-start(bf16[512,8]{0,1:T(8,128)(2,1)} %param.24) | copy-start | bytes 24580
  15.4 4.7 %copy-start.14 = (u32[32]{0:T(128)S(1)}, u32[32]{0:T(128)}, u32[]{:S(2)}) copy-start(u32[32]{0:T(128)} %constant.30) | copy-start | bytes 388
  15.4 44.5 %copy-start.13 = (f32[8]{0:T(128)S(1)}, f32[8]{0:T(128)}, u32[]{:S(2)}) copy-start(f32[8]{0:T(128)} %param.25) | copy-start | bytes 100
  15.4 44.5 %copy-start.12 = (f32[8]{0:T(128)S(1)}, f32[8]{0:T(128)}, u32[]{:S(2)}) copy-start(f32[8]{0:T(128)} %param.26) | copy-start | bytes 100
  15.4 81.0 %copy-start.1 = (f32[4,8,128,128]{3,2,1,0:T(8,128)S(1)}, f32[4,8,128,128]{3,2,1,0:T(8,128)}, u32[]{:S(2)}) copy-start(f32[4,8,128,128]{3,2,1,0:T(8,128)} %param.17) | copy-start | bytes 6291460
  19.7 130.2 %reduce-scatter.5.cloned.1.call-start = ((), (), s32[]{:S(2)}) async-start(), calls=%async_computation.2 | async-start | bytes 81920 | tf_op jit(solution)/shard_map/reduce_scatter | solution.py:108
  97.7 1.3 copy-start.2
  97.7 1.8 copy-start.11
  97.7 32.4 %copy-start.5 = (bf16[1024,512]{1,0:T(8,128)(2,1)S(1)}, bf16[1024,512]{1,0:T(8,128)(2,1)}, u32[]{:S(2)}) copy-start(bf16[1024,512]{1,0:T(8,128)(2,1)} %param.28) | copy-start | bytes 3145732
  97.7 52.2 %copy-start.7 = (bf16[32,128]{1,0:T(8,128)(2,1)S(1)}, bf16[32,128]{1,0:T(8,128)(2,1)}, u32[]{:S(2)}) copy-start(bf16[32,128]{1,0:T(8,128)(2,1)} %param.16) | copy-start | bytes 24580
  97.8 58.0 %copy-start.10 = (f32[512]{0:T(512)S(1)}, f32[512]{0:T(512)}, u32[]{:S(2)}) copy-start(f32[512]{0:T(512)} %param.29) | copy-start | bytes 6148
  131.1 99.6 %all-reduce.12.cloned.1.call-start = ((), (), s32[]{:S(2)}) async-start(), calls=%async_computation.3 | async-start | bytes 524288 | tf_op jit(solution)/shard_map/psum | solution.py:113
  159.5 94.1 %reduce-scatter.7.cloned.1.call-start = ((), (), s32[]{:S(2)}) async-start(), calls=%async_computation.4 | async-start | bytes 163840
Sparse Core Ops, SparseCore 0:
  19.8 75.3 all-reduce.13
  131.2 18.6 reduce-scatter.4
  159.7 71.0 all-reduce.11
  234.8 18.8 reduce-scatter.6
where the time goes:
time: 262 us
  waiting for transfers between devices  123 us (47%)
  blocking collectives  102 us (39%)
  matrix products  14.7 us (6%)
  between operations  14.6 us (6%)
  other arithmetic  3.95 us (2%)
  local copies, waits for them, and re-layouts  3.53 us (1%)
    unnamed x6, waiting for transfers between devices  54.3 us
    psum x1, waiting for transfers between devices, shards(): lax.psum(up_part.astype(jnp.bfloat16), 'kv').astype(jnp.float32)  49.6 us
    unnamed x1, blocking collectives  38.5 us
    all_gather x1, blocking collectives, shards(): lax.all_gather(heads_out, 'kv', axis=0, tiled=True)  30.5 us
    psum x1, blocking collectives, shards(): lax.psum(squares_mix.astype(jnp.bfloat16), 'kv').astype(jnp.float32)  21.4 us
    reduce_scatter x1, waiting for transfers between devices, shards(): lax.psum_scatter(attn_rows, 'tp', scatter_dimension=1, tiled=True)  18.8 us
    all_gather x2, blocking collectives, gathered_rows(): gathered = lax.all_gather(stream, 'tp', axis=1, tiled=True)  11.6 us
    dot_general x6, matrix products, product(): return jnp.dot(scaled, weight, preferred_element_type=jnp.float32)  6.11 us
  transfers between devices with their start and end apart: 4, of which 4 were waited for; matrix products, arithmetic and copies ran while one was open for 0% of the time, Pallas kernels for 0%

commit v1 on v0

v1 whole, which is shorter than its diff:
```python
import functools

import jax
import jax.numpy as jnp
from jax import lax
from jax.experimental import pallas as pl
from jax.experimental.pallas import tpu as pltpu
from jax.sharding import PartitionSpec as P

MESH = pl.DeviceIdType.MESH
F32 = jnp.float32
BF16 = jnp.bfloat16
epsilon = 1e-06
LANES = 128
CHUNKS = 2


def silu(x):
    return x * jax.nn.sigmoid(x)


def layer_kernel(
    nkv, ntp,
    stream_h, state_h, again_h, qw_h, kw_h, vw_h, gw_h, bw_h, dw_h, dlog_h, dshift_h, hgain_h,
    ow_h, mgain_h, uw_h, dn_h,
    out_v, next_h,
    stream_v, state_v, again_v, proj_v, bw_v, dw_v, dlog_v, dshift_v, hgain_v, ow_v, mgain_v, uw_v, dn_v,
    next_v, sbuf, psend, precv, bsend, brecv, y_v, dec_v, beta_v, ro_v, hbuf, abuf, mid_v, qbuf,
    usend, urecv, hidbuf, dsend, drecv,
    lsem, s_send, s_recv, p_send, p_recv, b_send, b_recv, h_send, h_recv, a_send, a_recv,
    q_send, q_recv, u_send, u_recv, f_send, f_recv, d_send, d_recv,
):
    kv = lax.axis_index("kv")
    tp = lax.axis_index("tp")
    rows, width = stream_v.shape
    depth = again_v.shape[1]
    model = depth * nkv
    vals = proj_v.shape[2]
    seqs, heads, hd, _ = state_v.shape
    cw = vals // CHUNKS

    def kv_to(d):
        return lax.rem(kv + d, nkv)

    def kv_from(d):
        return lax.rem(kv + nkv - d, nkv)

    def tp_to(d):
        return lax.rem(tp + d, ntp)

    def tp_from(d):
        return lax.rem(tp + ntp - d, ntp)

    pending = []

    def send(src, dst, ssem, rsem, axis, peer):
        copy = pltpu.make_async_remote_copy(
            src_ref=src, dst_ref=dst, send_sem=ssem, recv_sem=rsem,
            device_id={axis: peer}, device_id_type=MESH,
        )
        copy.start()
        pending.append(copy)
        return copy

    used = [0]

    def load(src, dst):
        copy = pltpu.make_async_copy(src, dst, lsem.at[used[0]])
        used[0] += 1
        copy.start()
        return copy

    c_stream = load(stream_h, stream_v)
    c_again = load(again_h, again_v)
    c_small = [
        load(a, b)
        for a, b in ((bw_h, bw_v), (dw_h, dw_v), (dlog_h, dlog_v), (dshift_h, dshift_v), (hgain_h, hgain_v), (mgain_h, mgain_v))
    ]
    c_proj = []
    for c in range(CHUNKS):
        cols = pl.ds(c * cw, cw)
        c_proj.append([load(w.at[:, cols], proj_v.at[t, :, cols]) for t, w in enumerate((qw_h, kw_h, vw_h, gw_h))])
    c_state = load(state_h, state_v)

    barrier = pltpu.get_barrier_semaphore()
    for d in range(1, nkv):
        pl.semaphore_signal(barrier, inc=1, device_id={"kv": kv_to(d)}, device_id_type=MESH)
    for d in range(1, ntp):
        pl.semaphore_signal(barrier, inc=1, device_id={"tp": tp_to(d)}, device_id_type=MESH)
    pl.semaphore_wait(barrier, nkv + ntp - 2)

    c_stream.wait()
    for d in range(1, ntp):
        send(stream_v, sbuf.at[tp], s_send.at[d], s_recv.at[d], "tp", tp_to(d))
    sbuf[tp] = stream_v[...]
    c_again.wait()
    for copy in c_small:
        copy.wait()
    for d in range(1, ntp):
        pltpu.make_async_remote_copy(
            src_ref=stream_v, dst_ref=sbuf.at[tp_from(d)], send_sem=s_send.at[d], recv_sem=s_recv.at[d],
            device_id={"tp": tp_to(d)}, device_id_type=MESH,
        ).wait_recv()
    full = jnp.concatenate([sbuf[s].astype(F32) for s in range(ntp)], axis=1)
    squares = jnp.sum(full * full, axis=1, keepdims=True)
    scaled = (full * again_v[...]).astype(BF16)

    beta_part = jnp.dot(scaled, bw_v[...], preferred_element_type=F32)
    decay_part = jnp.dot(scaled, dw_v[...], preferred_element_type=F32)
    square_part = jnp.broadcast_to(squares, (rows, heads))
    for j in range(nkv):
        part = slice(j * seqs, (j + 1) * seqs)
        bsend[j] = jnp.concatenate([beta_part[part], decay_part[part], square_part[part], square_part[part]], axis=0)
    b_copies = [
        send(bsend.at[kv_to(d)], brecv.at[d], b_send.at[d], b_recv.at[d], "kv", kv_to(d)) for d in range(1, nkv)
    ]
    p_copies = []
    for c in range(CHUNKS):
        for copy in c_proj[c]:
            copy.wait()
        parts = [
            jnp.dot(scaled, proj_v[t, :, c * cw : (c + 1) * cw], preferred_element_type=F32) for t in range(4)
        ]
        for j in range(nkv):
            part = slice(j * seqs, (j + 1) * seqs)
            psend[c, j] = jnp.concatenate([p[part] for p in parts], axis=0).astype(BF16)
        p_copies.append([
            send(psend.at[c, kv_to(d)], precv.at[c, d], p_send.at[c, d], p_recv.at[c, d], "kv", kv_to(d))
            for d in range(1, nkv)
        ])

    c_out = load(ow_h, ow_v)
    c_up = load(uw_h, uw_v)
    c_down = load(dn_h, dn_v)

    small = bsend[kv]
    for d in range(1, nkv):
        b_copies[d - 1].wait_recv()
        small = small + brecv[d]
    factor = lax.rsqrt(small[2 * seqs : 3 * seqs, 0:1] / model + epsilon)
    beta = jax.nn.sigmoid(small[0:seqs] * factor)
    decay_in = small[seqs : 2 * seqs] * factor + dshift_v[...]
    decay = jnp.exp(-jnp.exp(dlog_v[...]) * jax.nn.softplus(decay_in))
    for h in range(heads):
        dec_v[h * seqs : (h + 1) * seqs, :] = jnp.broadcast_to(decay[:, h : h + 1], (seqs, hd))
        beta_v[h * seqs : (h + 1) * seqs, :] = jnp.broadcast_to(beta[:, h : h + 1], (seqs, hd))
    kinds = 4 * seqs
    factor_rows = jnp.concatenate([factor] * 4, axis=0)
    kind = lax.broadcasted_iota(jnp.int32, (kinds, 1), 0) // seqs
    c_state.wait()
    groups = kinds // seqs
    per_group = heads // groups
    heads_chunk = cw // hd
    for c in range(CHUNKS):
        total = psend[c, kv].astype(F32)
        for d in range(1, nkv):
            p_copies[c][d - 1].wait_recv()
            total = total + precv[c, d].astype(F32)
        tall = []
        for hh in range(heads_chunk):
            x = silu(total[:, hh * hd : (hh + 1) * hd] * factor_rows)
            norm = lax.rsqrt(jnp.sum(x * x, axis=1, keepdims=True) + epsilon)
            scale = jnp.where(kind == 0, norm * hd ** (-0.5), jnp.where(kind == 1, norm, 1.0))
            tall.append(x * scale)
        y = jnp.concatenate(tall, axis=0)
        y_v[c] = y
        y_t = y.T
        for hh in range(heads_chunk):
            h = c * heads_chunk + hh
            for b in range(seqs):
                row = h * seqs + b
                base = hh * kinds + b
                q_col = y_t[:, base : base + 1]
                k_col = y_t[:, base + seqs : base + seqs + 1]
                kept = state_v[b, h] * dec_v[row : row + 1, :]
                recalled = jnp.sum(kept * k_col, axis=0, keepdims=True)
                value = y_v[c, base + 2 * seqs : base + 2 * seqs + 1, :]
                correction = beta_v[row : row + 1, :] * (value - recalled)
                after = kept + k_col * correction
                next_v[b, h] = after
                group, place = h // per_group, h % per_group
                at = place * kinds + group * seqs + b
                ro_v[at : at + 1, :] = jnp.sum(after * q_col, axis=0, keepdims=True)
    c_next = pltpu.make_async_copy(next_v, next_h, lsem.at[used[0]])
    c_next.start()
    used[0] += 1

    pieces = []
    for place in range(per_group):
        readout = ro_v[place * kinds : (place + 1) * kinds, :]
        gates = []
        for group in range(groups):
            h = group * per_group + place
            base = (h % heads_chunk) * kinds + 3 * seqs
            gates.append(y_v[h // heads_chunk, base : base + seqs, :])
        gate = jnp.concatenate(gates, axis=0)
        normed = readout * lax.rsqrt(jnp.mean(readout * readout, axis=1, keepdims=True) + epsilon)
        pieces.append(normed * hgain_v[...] * gate)
    hbuf[kv] = jnp.concatenate(pieces, axis=1).astype(BF16)
    for d in range(1, nkv):
        send(hbuf.at[kv], hbuf.at[kv], h_send.at[d], h_recv.at[d], "kv", kv_to(d))
    c_out.wait()
    for d in range(1, nkv):
        pltpu.make_async_remote_copy(
            src_ref=hbuf.at[kv], dst_ref=hbuf.at[kv_from(d)], send_sem=h_send.at[d], recv_sem=h_recv.at[d],
            device_id={"kv": kv_to(d)}, device_id_type=MESH,
        ).wait_recv()
    blocks = [hbuf[s].astype(F32) for s in range(nkv)]
    ordered = jnp.concatenate(
        [
            jnp.concatenate([block[g * seqs : (g + 1) * seqs] for block in blocks], axis=0)
            for g in range(groups)
        ],
        axis=1,
    ).astype(BF16)
    attn_part = jnp.dot(ordered, ow_v[...], preferred_element_type=F32)

    abuf[tp] = attn_part.astype(BF16)
    for d in range(1, ntp):
        send(abuf.at[tp], abuf.at[tp], a_send.at[d], a_recv.at[d], "tp", tp_to(d))
    for d in range(1, ntp):
        pltpu.make_async_remote_copy(
            src_ref=abuf.at[tp], dst_ref=abuf.at[tp_from(d)], send_sem=a_send.at[d], recv_sem=a_recv.at[d],
            device_id={"tp": tp_to(d)}, device_id_type=MESH,
        ).wait_recv()
    attn = abuf[0].astype(F32)
    for s in range(1, ntp):
        attn = attn + abuf[s].astype(F32)
    stream_all = jnp.concatenate([sbuf[s].astype(F32) for s in range(ntp)], axis=1)
    middle = (stream_all + attn).astype(BF16).astype(F32)
    for s in range(ntp):
        mid_v[s] = middle[:, s * width : (s + 1) * width]
    square_mix = jnp.sum(middle * middle, axis=1, keepdims=True)
    lanes = qbuf.shape[2]
    diagonal = lax.broadcasted_iota(jnp.int32, (rows, lanes), 0) == lax.broadcasted_iota(jnp.int32, (rows, lanes), 1)
    flat = jnp.sum(jnp.where(diagonal, square_mix, 0.0), axis=0, keepdims=True)
    qbuf[0] = jnp.broadcast_to(flat, qbuf.shape[1:])
    q_copies = [
        send(qbuf.at[0], qbuf.at[d], q_send.at[d], q_recv.at[d], "kv", kv_to(d)) for d in range(1, nkv)
    ]
    mixed = (middle * mgain_v[...]).astype(BF16)

    c_up.wait()
    uw = uw_v.shape[1] // nkv
    u_copies = []
    if uw % LANES == 0:
        for d in range(1, nkv + 1):
            peer = kv_to(d)
            cols = pl.ds(pl.multiple_of(peer * uw, LANES), uw)
            part = jnp.dot(mixed, uw_v[:, cols], preferred_element_type=F32)
            if d < nkv:
                usend[d] = part.astype(BF16)
                u_copies.append(send(usend.at[d], urecv.at[d], u_send.at[d], u_recv.at[d], "kv", peer))
            else:
                own = part
    else:
        part = jnp.dot(mixed, uw_v[...], preferred_element_type=F32).astype(BF16)
        for j in range(nkv):
            usend[j] = part[:, j * uw : (j + 1) * uw]
        for d in range(1, nkv):
            u_copies.append(send(usend.at[kv_to(d)], urecv.at[d], u_send.at[d], u_recv.at[d], "kv", kv_to(d)))
        own = usend[kv].astype(F32)
    for d in range(1, nkv):
        q_copies[d - 1].wait_recv()
    total_flat = jnp.sum(qbuf[...], axis=0)[0:1, :]
    total_mix = jnp.sum(jnp.where(diagonal, total_flat, 0.0), axis=1, keepdims=True)
    factor_mix = lax.rsqrt(total_mix / model + epsilon)
    for d in range(1, nkv):
        u_copies[d - 1].wait_recv()
        own = own + urecv[d].astype(F32)
    hidden = jnp.square(jnp.maximum(own * factor_mix, 0.0)).astype(BF16)
    hidbuf[0] = hidden
    f_copies = [
        send(hidbuf.at[0], hidbuf.at[d], f_send.at[d], f_recv.at[d], "kv", kv_to(d)) for d in range(1, nkv)
    ]
    c_down.wait()
    down = None
    for d in range(nkv):
        if d > 0:
            f_copies[d - 1].wait_recv()
        units = pl.ds(pl.multiple_of(kv_from(d) * uw, uw), uw)
        term = jnp.dot(hidbuf[d], dn_v[units, :], preferred_element_type=F32)
        down = term if down is None else down + term
    for s in range(ntp):
        dsend[s] = down[:, s * width : (s + 1) * width].astype(BF16)
    d_copies = [
        send(dsend.at[tp_to(d)], drecv.at[d], d_send.at[d], d_recv.at[d], "tp", tp_to(d)) for d in range(1, ntp)
    ]
    result = dsend[tp].astype(F32)
    for d in range(1, ntp):
        d_copies[d - 1].wait_recv()
        result = result + drecv[d].astype(F32)
    out_v[...] = (mid_v[tp] + result).astype(BF16)
    for copy in pending:
        copy.wait_send()
    c_next.wait()


def layer(nkv, ntp, stream, state, again, qw, kw, vw, gw, bw, dw, dlog, dshift, hgain, ow, mgain, uw, dn):
    rows, width = stream.shape
    depth = again.shape[0]
    vals = qw.shape[1]
    seqs, heads, hd, _ = state.shape
    cw = vals // CHUNKS
    kinds = 4 * seqs
    hidden = uw.shape[1]
    unit = hidden // nkv
    lanes = -(-rows // LANES) * LANES
    cols = ow.shape[1]
    again, mgain, dlog, dshift, hgain = (v.reshape(1, -1) for v in (again, mgain, dlog, dshift, hgain))
    operands = (stream, state, again, qw, kw, vw, gw, bw, dw, dlog, dshift, hgain, ow, mgain, uw, dn)
    vmem, dma = pltpu.VMEM, pltpu.SemaphoreType.DMA

    def like(x):
        return vmem(x.shape, x.dtype)

    scratch = [
        like(stream), like(state), like(again), vmem((4, depth, vals), BF16), like(bw), like(dw), like(dlog),
        like(dshift), like(hgain), like(ow), like(mgain), like(uw), like(dn),
        like(state),
        vmem((ntp, rows, width), BF16),
        vmem((CHUNKS, nkv, kinds, cw), BF16), vmem((CHUNKS, nkv, kinds, cw), BF16),
        vmem((nkv, kinds, heads), F32), vmem((nkv, kinds, heads), F32),
        vmem((CHUNKS, heads // CHUNKS * kinds, hd), F32),
        vmem((heads * seqs, hd), F32), vmem((heads * seqs, hd), F32), vmem((heads * seqs, hd), F32),
        vmem((nkv, kinds, vals * seqs // kinds), BF16),
        vmem((ntp, rows, cols), BF16),
        vmem((ntp, rows, width), F32),
        vmem((nkv, 8, lanes), F32),
        vmem((nkv, rows, unit), BF16), vmem((nkv, rows, unit), BF16), vmem((nkv, rows, unit), BF16),
        vmem((ntp, rows, width), BF16), vmem((ntp, rows, width), BF16),
        dma((8 + 4 * CHUNKS + 5,)),
        dma((ntp,)), dma((ntp,)),
        dma((CHUNKS, nkv)), dma((CHUNKS, nkv)),
        dma((nkv,)), dma((nkv,)), dma((nkv,)), dma((nkv,)),
        dma((ntp,)), dma((ntp,)),
        dma((nkv,)), dma((nkv,)), dma((nkv,)), dma((nkv,)), dma((nkv,)), dma((nkv,)),
        dma((ntp,)), dma((ntp,)),
    ]
    return pl.pallas_call(
        functools.partial(layer_kernel, nkv, ntp),
        out_shape=(
            jax.ShapeDtypeStruct((rows, width), BF16),
            jax.ShapeDtypeStruct(state.shape, state.dtype),
        ),
        in_specs=[pl.BlockSpec(memory_space=pl.ANY)] * len(operands),
        out_specs=(pl.BlockSpec(memory_space=pltpu.VMEM), pl.BlockSpec(memory_space=pl.ANY)),
        scratch_shapes=scratch,
        compiler_params=pltpu.CompilerParams(
            collective_id=0, has_side_effects=True, vmem_limit_bytes=60 * 1024 * 1024
        ),
    )(*operands)


def solution(mesh):
    in_specs = (
        P(None, ("kv", "tp")),
        P("kv", "tp", None, None),
        P("kv"),
        P("kv", "tp"),
        P("kv", "tp"),
        P("kv", "tp"),
        P("kv", "tp"),
        P("kv", "tp"),
        P("kv", "tp"),
        P("tp"),
        P("tp"),
        P(),
        P("tp", "kv"),
        P("kv"),
        P("kv", "tp"),
        P("tp", "kv"),
    )
    out_specs = (P(None, ("kv", "tp")), P("kv", "tp", None, None))
    shards = functools.partial(layer, mesh.shape["kv"], mesh.shape["tp"])
    return jax.shard_map(shards, mesh=mesh, in_specs=in_specs, out_specs=out_specs, check_vma=False)
```

time: 262 us -> 55.3 us (0.21)
  waiting for transfers between devices: 123 us -> 0 us
  blocking collectives: 102 us -> 0 us
  Pallas kernels: 0 us -> 46.9 us
  matrix products: 14.7 us -> 0 us
  between operations: 14.6 us -> 0.64 us
  other arithmetic: 3.95 us -> 0 us
  local copies, waits for them, and re-layouts: 3.53 us -> 7.42 us
    unnamed x6 -> x0, waiting for transfers between devices: 54.3 us -> none
    psum x1 -> x0, waiting for transfers between devices: 49.6 us -> none  [shards(): lax.psum(up_part.astype(jnp.bfloat16), 'kv').astype(jnp.float32)]
    pallas_call x0 -> x1, Pallas kernels: none -> 46.9 us  [layer(): pl.pallas_call(functools.partial(layer_kernel, nkv, ntp), out_shape=(jax....]
    all_gather x3 -> x0, blocking collectives: 42.2 us -> none  [the longest x1 30.5 us: shards(): lax.all_gather(heads_out, 'kv', axis=0, tiled=True)]
    unnamed x1 -> x0, blocking collectives: 38.5 us -> none
    psum x1 -> x0, blocking collectives: 21.4 us -> none  [shards(): lax.psum(squares_mix.astype(jnp.bfloat16), 'kv').astype(jnp.float32)]
    reduce_scatter x1 -> x0, waiting for transfers between devices: 18.8 us -> none  [shards(): lax.psum_scatter(attn_rows, 'tp', scatter_dimension=1, tiled=True)]
    dot_general x11 -> x0, matrix products: 14.7 us -> none  [the longest x6 6.11 us: product(): return jnp.dot(scaled, weight, preferred_element_type=jnp.float32)]
  transfers between devices with their start and end apart: 4 -> 0, of which waited for: 4 -> 0; matrix products, arithmetic and copies ran while one was open for 0% -> 0% of each run, Pallas kernels for 0% -> 0%
where the time goes in v1:
time: 55.3 us; the launch traced here: 55 us
  Pallas kernels  46.9 us (85%)
  local copies, waits for them, and re-layouts  7.42 us (13%)
  between operations  0.64 us (1%)
    pallas_call x1, Pallas kernels, layer(): pl.pallas_call(functools.partial(layer_kernel, nkv, ntp), out_shape=(jax....  46.9 us
    unnamed x4, local copies, waits for them, and re-layouts  7.42 us

profile of v1, /device:TPU:0, one launch (start us, length us, event | category | flops | bytes accessed | tf_op | source)
XLA Modules:
  0.0 55.0 jit_solution(915728962414528162)
XLA Ops:
  0.6 1.5 %copy.18.bw_h = bf16[512,8]{1,0:T(8,128)(2,1)} copy(bf16[512,8]{0,1:T(8,128)(2,1)} %param.23) | data formatting | bytes 16384 | tf_op args[7]
  2.1 1.5 %copy.19.dw_h = bf16[512,8]{1,0:T(8,128)(2,1)} copy(bf16[512,8]{0,1:T(8,128)(2,1)} %param.24) | data formatting | bytes 16384 | tf_op args[8]
  3.6 46.9 %shard_map.167 = (bf16[32,128]{1,0:T(8,128)(2,1)}, f32[4,8,128,128]{3,2,1,0:T(8,128)}) custom-call(bf16[32,128]{1,0:T(8,128)(2,1)} %stream_h.1, f32[4,8,128,128]{3,2,1,0:T(8,128)} %state_h.1, f32[1,512]{1,0:T(1,128)} %bitcast.5, bf16[512,1024]{1,0:T(8,128)(2,1)} %qw_h.1, bf16[512,1024]{1,0:T(8,128)(2,1)} %kw_h.1, bf16[512,1024]{1,0:T(8,128)(2,1)} %vw_h.1, ...), custom_call_target="tpu_custom_call" | custom-call | tf_op jit(solution)/shard_map/pallas_call | solution.py:340
  50.5 1.3 %copy.22 = bf16[32,128]{1,0:T(8,128)(2,1)} copy(bf16[32,128]{1,0:T(8,128)(2,1)} %get-tuple-element.4) | data formatting | bytes 16384
  51.8 3.1 %copy.23 = f32[4,8,128,128]{3,2,1,0:T(8,128)} copy(f32[4,8,128,128]{3,2,1,0:T(8,128)} %get-tuple-element.5) | data formatting | bytes 4194304

commit v2 on v1

--- a/solution.py
+++ b/solution.py
@@ -19,13 +19,17 @@
     return x * jax.nn.sigmoid(x)
 
 
+def across(a, b):
+    return lax.dot_general(a, b, (((1,), (1,)), ((), ())), preferred_element_type=F32)
+
+
 def layer_kernel(
     nkv, ntp,
     stream_h, state_h, again_h, qw_h, kw_h, vw_h, gw_h, bw_h, dw_h, dlog_h, dshift_h, hgain_h,
     ow_h, mgain_h, uw_h, dn_h,
-    out_v, next_h,
+    out_v, next_v,
     stream_v, state_v, again_v, proj_v, bw_v, dw_v, dlog_v, dshift_v, hgain_v, ow_v, mgain_v, uw_v, dn_v,
-    next_v, sbuf, psend, precv, bsend, brecv, y_v, dec_v, beta_v, ro_v, hbuf, abuf, mid_v, qbuf,
+    sbuf, psend, precv, bsend, brecv, y_v, dec_v, beta_v, ro_v, hbuf, abuf, mid_v, qbuf,
     usend, urecv, hidbuf, dsend, drecv,
     lsem, s_send, s_recv, p_send, p_recv, b_send, b_recv, h_send, h_recv, a_send, a_recv,
     q_send, q_recv, u_send, u_recv, f_send, f_recv, d_send, d_recv,
@@ -39,11 +43,22 @@
     seqs, heads, hd, _ = state_v.shape
     cw = vals // CHUNKS
 
+    paired = nkv & (nkv - 1) == 0
+    far_first = range(nkv - 1, 0, -1)
+
+    def flipped(d):
+        peer, bit = kv, 1
+        while bit < nkv:
+            if d & bit:
+                peer = peer + bit * (1 - 2 * ((kv // bit) % 2))
+            bit *= 2
+        return peer
+
     def kv_to(d):
-        return lax.rem(kv + d, nkv)
+        return flipped(d) if paired else lax.rem(kv + d, nkv)
 
     def kv_from(d):
-        return lax.rem(kv + nkv - d, nkv)
+        return flipped(d) if paired else lax.rem(kv + nkv - d, nkv)
 
     def tp_to(d):
         return lax.rem(tp + d, ntp)
@@ -105,15 +120,15 @@
     squares = jnp.sum(full * full, axis=1, keepdims=True)
     scaled = (full * again_v[...]).astype(BF16)
 
-    beta_part = jnp.dot(scaled, bw_v[...], preferred_element_type=F32)
-    decay_part = jnp.dot(scaled, dw_v[...], preferred_element_type=F32)
+    beta_part = across(scaled, bw_v[...])
+    decay_part = across(scaled, dw_v[...])
     square_part = jnp.broadcast_to(squares, (rows, heads))
     for j in range(nkv):
         part = slice(j * seqs, (j + 1) * seqs)
         bsend[j] = jnp.concatenate([beta_part[part], decay_part[part], square_part[part], square_part[part]], axis=0)
-    b_copies = [
-        send(bsend.at[kv_to(d)], brecv.at[d], b_send.at[d], b_recv.at[d], "kv", kv_to(d)) for d in range(1, nkv)
-    ]
+    b_copies = {
+        d: send(bsend.at[kv_to(d)], brecv.at[d], b_send.at[d], b_recv.at[d], "kv", kv_to(d)) for d in far_first
+    }
     p_copies = []
     for c in range(CHUNKS):
         for copy in c_proj[c]:
@@ -124,10 +139,10 @@
         for j in range(nkv):
             part = slice(j * seqs, (j + 1) * seqs)
             psend[c, j] = jnp.concatenate([p[part] for p in parts], axis=0).astype(BF16)
-        p_copies.append([
-            send(psend.at[c, kv_to(d)], precv.at[c, d], p_send.at[c, d], p_recv.at[c, d], "kv", kv_to(d))
-            for d in range(1, nkv)
-        ])
+        p_copies.append({
+            d: send(psend.at[c, kv_to(d)], precv.at[c, d], p_send.at[c, d], p_recv.at[c, d], "kv", kv_to(d))
+            for d in far_first
+        })
 
     c_out = load(ow_h, ow_v)
     c_up = load(uw_h, uw_v)
@@ -135,7 +150,7 @@
 
     small = bsend[kv]
     for d in range(1, nkv):
-        b_copies[d - 1].wait_recv()
+        b_copies[d].wait_recv()
         small = small + brecv[d]
     factor = lax.rsqrt(small[2 * seqs : 3 * seqs, 0:1] / model + epsilon)
     beta = jax.nn.sigmoid(small[0:seqs] * factor)
@@ -154,7 +169,7 @@
     for c in range(CHUNKS):
         total = psend[c, kv].astype(F32)
         for d in range(1, nkv):
-            p_copies[c][d - 1].wait_recv()
+            p_copies[c][d].wait_recv()
             total = total + precv[c, d].astype(F32)
         tall = []
         for hh in range(heads_chunk):
@@ -181,9 +196,6 @@
                 group, place = h // per_group, h % per_group
                 at = place * kinds + group * seqs + b
                 ro_v[at : at + 1, :] = jnp.sum(after * q_col, axis=0, keepdims=True)
-    c_next = pltpu.make_async_copy(next_v, next_h, lsem.at[used[0]])
-    c_next.start()
-    used[0] += 1
 
     pieces = []
     for place in range(per_group):
@@ -197,7 +209,7 @@
         normed = readout * lax.rsqrt(jnp.mean(readout * readout, axis=1, keepdims=True) + epsilon)
         pieces.append(normed * hgain_v[...] * gate)
     hbuf[kv] = jnp.concatenate(pieces, axis=1).astype(BF16)
-    for d in range(1, nkv):
+    for d in far_first:
         send(hbuf.at[kv], hbuf.at[kv], h_send.at[d], h_recv.at[d], "kv", kv_to(d))
     c_out.wait()
     for d in range(1, nkv):
@@ -235,49 +247,49 @@
     diagonal = lax.broadcasted_iota(jnp.int32, (rows, lanes), 0) == lax.broadcasted_iota(jnp.int32, (rows, lanes), 1)
     flat = jnp.sum(jnp.where(diagonal, square_mix, 0.0), axis=0, keepdims=True)
     qbuf[0] = jnp.broadcast_to(flat, qbuf.shape[1:])
-    q_copies = [
-        send(qbuf.at[0], qbuf.at[d], q_send.at[d], q_recv.at[d], "kv", kv_to(d)) for d in range(1, nkv)
-    ]
+    q_copies = {
+        d: send(qbuf.at[0], qbuf.at[d], q_send.at[d], q_recv.at[d], "kv", kv_to(d)) for d in far_first
+    }
     mixed = (middle * mgain_v[...]).astype(BF16)
 
     c_up.wait()
     uw = uw_v.shape[1] // nkv
-    u_copies = []
+    u_copies = {}
     if uw % LANES == 0:
-        for d in range(1, nkv + 1):
+        for d in (*far_first, 0):
             peer = kv_to(d)
             cols = pl.ds(pl.multiple_of(peer * uw, LANES), uw)
             part = jnp.dot(mixed, uw_v[:, cols], preferred_element_type=F32)
-            if d < nkv:
+            if d > 0:
                 usend[d] = part.astype(BF16)
-                u_copies.append(send(usend.at[d], urecv.at[d], u_send.at[d], u_recv.at[d], "kv", peer))
+                u_copies[d] = send(usend.at[d], urecv.at[d], u_send.at[d], u_recv.at[d], "kv", peer)
             else:
                 own = part
     else:
         part = jnp.dot(mixed, uw_v[...], preferred_element_type=F32).astype(BF16)
         for j in range(nkv):
             usend[j] = part[:, j * uw : (j + 1) * uw]
-        for d in range(1, nkv):
-            u_copies.append(send(usend.at[kv_to(d)], urecv.at[d], u_send.at[d], u_recv.at[d], "kv", kv_to(d)))
+        for d in far_first:
+            u_copies[d] = send(usend.at[kv_to(d)], urecv.at[d], u_send.at[d], u_recv.at[d], "kv", kv_to(d))
         own = usend[kv].astype(F32)
     for d in range(1, nkv):
-        q_copies[d - 1].wait_recv()
+        q_copies[d].wait_recv()
     total_flat = jnp.sum(qbuf[...], axis=0)[0:1, :]
     total_mix = jnp.sum(jnp.where(diagonal, total_flat, 0.0), axis=1, keepdims=True)
     factor_mix = lax.rsqrt(total_mix / model + epsilon)
     for d in range(1, nkv):
-        u_copies[d - 1].wait_recv()
+        u_copies[d].wait_recv()
         own = own + urecv[d].astype(F32)
     hidden = jnp.square(jnp.maximum(own * factor_mix, 0.0)).astype(BF16)
     hidbuf[0] = hidden
-    f_copies = [
-        send(hidbuf.at[0], hidbuf.at[d], f_send.at[d], f_recv.at[d], "kv", kv_to(d)) for d in range(1, nkv)
-    ]
+    f_copies = {
+        d: send(hidbuf.at[0], hidbuf.at[d], f_send.at[d], f_recv.at[d], "kv", kv_to(d)) for d in far_first
+    }
     c_down.wait()
     down = None
     for d in range(nkv):
         if d > 0:
-            f_copies[d - 1].wait_recv()
+            f_copies[d].wait_recv()
         units = pl.ds(pl.multiple_of(kv_from(d) * uw, uw), uw)
         term = jnp.dot(hidbuf[d], dn_v[units, :], preferred_element_type=F32)
         down = term if down is None else down + term
@@ -293,7 +305,6 @@
     out_v[...] = (mid_v[tp] + result).astype(BF16)
     for copy in pending:
         copy.wait_send()
-    c_next.wait()
 
 
 def layer(nkv, ntp, stream, state, again, qw, kw, vw, gw, bw, dw, dlog, dshift, hgain, ow, mgain, uw, dn):
@@ -308,6 +319,7 @@
     lanes = -(-rows // LANES) * LANES
     cols = ow.shape[1]
     again, mgain, dlog, dshift, hgain = (v.reshape(1, -1) for v in (again, mgain, dlog, dshift, hgain))
+    bw, dw = bw.T, dw.T
     operands = (stream, state, again, qw, kw, vw, gw, bw, dw, dlog, dshift, hgain, ow, mgain, uw, dn)
     vmem, dma = pltpu.VMEM, pltpu.SemaphoreType.DMA
 
@@ -317,7 +329,6 @@
     scratch = [
         like(stream), like(state), like(again), vmem((4, depth, vals), BF16), like(bw), like(dw), like(dlog),
         like(dshift), like(hgain), like(ow), like(mgain), like(uw), like(dn),
-        like(state),
         vmem((ntp, rows, width), BF16),
         vmem((CHUNKS, nkv, kinds, cw), BF16), vmem((CHUNKS, nkv, kinds, cw), BF16),
         vmem((nkv, kinds, heads), F32), vmem((nkv, kinds, heads), F32),
@@ -340,14 +351,14 @@
     return pl.pallas_call(
         functools.partial(layer_kernel, nkv, ntp),
         out_shape=(
-            jax.ShapeDtypeStruct((rows, width), BF16),
-            jax.ShapeDtypeStruct(state.shape, state.dtype),
+            pltpu.VMEM((rows, width), BF16),
+            pltpu.VMEM(state.shape, state.dtype),
         ),
-        in_specs=[pl.BlockSpec(memory_space=pl.ANY)] * len(operands),
-        out_specs=(pl.BlockSpec(memory_space=pltpu.VMEM), pl.BlockSpec(memory_space=pl.ANY)),
+        in_specs=[pl.BlockSpec(memory_space=pltpu.HBM)] * len(operands),
+        out_specs=(pl.BlockSpec(memory_space=pltpu.VMEM), pl.BlockSpec(memory_space=pltpu.VMEM)),
         scratch_shapes=scratch,
         compiler_params=pltpu.CompilerParams(
-            collective_id=0, has_side_effects=True, vmem_limit_bytes=60 * 1024 * 1024
+            collective_id=0, has_side_effects=True, vmem_limit_bytes=56 * 1024 * 1024
         ),
     )(*operands)
 

time: 55.3 us -> 48.4 us (0.88)
  local copies, waits for them, and re-layouts: 7.42 us -> 1.92 us
  Pallas kernels: 46.9 us -> 45.7 us
    unnamed x4 -> x2, local copies, waits for them, and re-layouts: 7.42 us -> 1.92 us
    pallas_call x1, Pallas kernels: 46.9 us -> 45.7 us  [layer(): pl.pallas_call(functools.partial(layer_kernel, nkv, ntp), out_shape=(pltp...]
where the time goes in v2:
time: 48.4 us; the launch traced here: 48.2 us
  Pallas kernels  45.7 us (94%)
  local copies, waits for them, and re-layouts  1.92 us (4%)
  between operations  0.65 us (1%)
    pallas_call x1, Pallas kernels, layer(): pl.pallas_call(functools.partial(layer_kernel, nkv, ntp), out_shape=(pltp...  45.7 us
    unnamed x2, local copies, waits for them, and re-layouts  1.92 us

profile of v2, /device:TPU:0, one launch (start us, length us, event | category | flops | bytes accessed | tf_op | source)
XLA Modules:
  0.0 48.2 jit_solution(13901271474255110660)
XLA Ops:
  0.6 45.7 %shard_map.167 = (bf16[32,128]{1,0:T(8,128)(2,1)S(1)}, f32[4,8,128,128]{3,2,1,0:T(8,128)S(1)}) custom-call(bf16[32,128]{1,0:T(8,128)(2,1)} %stream_h.1, f32[4,8,128,128]{3,2,1,0:T(8,128)} %state_h.1, f32[1,512]{1,0:T(1,128)} %bitcast.9, bf16[512,1024]{1,0:T(8,128)(2,1)} %qw_h.1, bf16[512,1024]{1,0:T(8,128)(2,1)} %kw_h.1, bf16[512,1024]{1,0:T(8,128)(2,1)} %vw_h.1, ...), custom_call_target="tpu_custom_call" | custom-call | tf_op jit(solution)/shard_map/pallas_call | solution.py:351
  46.3 0.6 %copy.20 = bf16[32,128]{1,0:T(8,128)(2,1)} copy(bf16[32,128]{1,0:T(8,128)(2,1)S(1)} %get-tuple-element.2) | data formatting | bytes 16384
  46.9 1.3 %copy.21 = f32[4,8,128,128]{3,2,1,0:T(8,128)} copy(f32[4,8,128,128]{3,2,1,0:T(8,128)S(1)} %get-tuple-element.3) | data formatting | bytes 4194304
